TPU v7x, 32 devices: a whole 2x2x4 slice. The times are simulated.
32 devices in a mesh: grp: 2 (over x), ep: 16 (over z, y, core).
Axes of the slice: x: 2, y: 2, z: 4, core: 2. Of those that a mesh axis runs over, the one named last changes fastest.
Arguments:
- tokens: bfloat16 [256, 2048], P(('grp', 'ep')), parts along dimension 0, may hold values from -6 to 6
- routes: int32 [256, 4], P(('grp', 'ep')), parts along dimension 0, may hold values from 0 to 15, all different within a row; in each aligned block of 8 rows (0 to 7, 8 to 15, ...) at most 4 rows name the same one
- gate_weights: float32 [256, 4], P(('grp', 'ep')), parts along dimension 0, may hold values from 0.1 to 1
- norm_gain: float32 [2048], replicated, may hold values from 0.1 to 1.9
- final_gain: float32 [2048], replicated, may hold values from 0.1 to 1.9
- w_gate: bfloat16 [16, 2048, 512], P('ep'), may hold values from -0.088388348 to 0.088388348
- w_up: bfloat16 [16, 2048, 512], P('ep'), may hold values from -0.088388348 to 0.088388348
- w_down: bfloat16 [16, 512, 2048], P('ep'), may hold values from -0.176776695 to 0.176776695
Outputs:
- mixed: bfloat16 [256, 2048], P('grp', 'ep'), parts along dimension 0
There are 2 independent parts, one for each index of `grp`. A program takes and returns all parts, laid end to end along the dimension named above; an argument that names none is the same for every part. Nothing has to cross between parts.
Inputs may be any that keep to these rules, and one draw needn't show every extreme that they name: `routes`: each row names 4 different experts; among the rows of one device no expert is named by more than 4 rows, and some expert reaches 4.
All inputs are finite; a program needn't handle non-finite values.
Results may differ from a plain program's by a relative error of at most 0.008.
Values may be sent and summed in bfloat16 or wider, within the bound.
A program may use at most 64 MiB of HBM per device.

v0:
```python
import jax
import jax.numpy as jnp
from jax import lax
from jax.sharding import PartitionSpec as P


def expert_rows(rows, w_gate, w_up, w_down):
    gate_val = jnp.dot(rows, w_gate[0], preferred_element_type=jnp.float32)
    up_val = jnp.dot(rows, w_up[0], preferred_element_type=jnp.float32)
    act = (jax.nn.silu(gate_val) * up_val).astype(jnp.bfloat16)
    return jnp.dot(act, w_down[0], preferred_element_type=jnp.float32).astype(jnp.bfloat16)


def shards(tokens, routes, gate_weights, norm_gain, final_gain, w_gate, w_up, w_down):
    epsilon = 1e-06
    width = tokens.shape[1]
    topk = routes.shape[1]
    group = lax.axis_size("ep")
    per_dev = tokens.shape[0]
    most = max(2, (2 * per_dev * topk + group - 1) // group)
    values = tokens.astype(jnp.float32)
    normed = (
        values * lax.rsqrt(jnp.mean(values * values, axis=1, keepdims=True) + epsilon) * norm_gain
    ).astype(jnp.bfloat16)
    slots = jnp.arange(most, dtype=jnp.int32)
    experts = jnp.arange(group, dtype=jnp.int32)
    match = (routes[:, :, None] == experts[None, None, :]).astype(jnp.float32)
    row_used = jnp.sum(match, axis=1)
    row_gate = jnp.sum(match * gate_weights[:, :, None], axis=1)
    order_pos = jnp.cumsum(row_used, axis=0).astype(jnp.int32) - 1
    select = jnp.transpose(row_used)[:, None, :] * (
        jnp.transpose(order_pos)[:, None, :] == slots[None, :, None]
    ).astype(jnp.float32)
    outgoing = jnp.einsum(
        "ecr,rd->ecd", select.astype(jnp.bfloat16), normed, preferred_element_type=jnp.float32
    ).astype(jnp.bfloat16)
    received = lax.all_to_all(outgoing, "ep", split_axis=0, concat_axis=0, tiled=True)
    count = received.shape[1]
    result = expert_rows(received.reshape(-1, width), w_gate, w_up, w_down)
    returned = lax.all_to_all(
        result.reshape(group, count, width), "ep", split_axis=0, concat_axis=0, tiled=True
    )
    weights = select * jnp.transpose(row_gate)[:, None, :]
    combined = jnp.einsum(
        "ecr,ecd->rd", weights, returned.astype(jnp.float32), precision=lax.Precision.HIGHEST
    )
    scale = lax.rsqrt(jnp.mean(combined * combined, axis=1, keepdims=True) + epsilon)
    finished = (combined * scale * final_gain).astype(jnp.bfloat16)
    return lax.all_to_all(finished, "ep", split_axis=1, concat_axis=0, tiled=True)


def solution(mesh):
    in_specs = (
        P(("grp", "ep"), None),
        P(("grp", "ep"), None),
        P(("grp", "ep"), None),
        P(),
        P(),
        P("ep", None, None),
        P("ep", None, None),
        P("ep", None, None),
    )
    out_specs = P("grp", "ep")
    return jax.shard_map(shards, mesh=mesh, in_specs=in_specs, out_specs=out_specs, check_vma=False)
```

profile of v0, /device:TPU:0, one launch (start us, length us, event | category | flops | bytes accessed | tf_op | source)
XLA Modules:
  0.0 48.4 jit_solution(1577302397109004149)
XLA Ops:
  0.0 0.0 copy-start
  0.0 1.0 %fusion.19 = f32[8]{0:T(128)S(1)} fusion(bf16[8,2048]{1,0:T(8,128)(2,1)} %param.8), kind=kLoop, calls=%fused_computation.18 | loop fusion | flops 49144 | bytes 32800 | tf_op jit(solution)/shard_map/reduce_sum | solution.py:23
  1.0 0.8 %select_reduce_fusion = (f32[8,16]{1,0:T(8,128)S(1)}, f32[8,16]{1,0:T(8,128)S(1)}) fusion(f32[8,4]{0,1:T(4,128)} %param.10, s32[8,4]{0,1:T(4,128)} %param.9), kind=kLoop, calls=%fused_computation.30 | loop fusion | flops 2304 | bytes 1280 | tf_op jit(solution)/shard_map/reduce_sum | solution.py:29
  1.9 1.0 %convolution_convert_fusion.1 = bf16[16,4,2048]{2,0,1:T(8,128)(2,1)S(1)} fusion(bf16[8,2048]{1,0:T(8,128)(2,1)} %param.8, f32[2048]{0:T(1024)} %param.11, f32[8]{0:T(128)S(1)} %add_rsqrt_fusion.1, f32[16,8]{0,1:T(8,128)S(1)} %bitcast.32, s32[16,8]{0,1:T(8,128)S(1)} %add_bitcast_fusion), kind=kOutput, calls=%fused_computation.1 | convolution fusion | flops 2294784 | bytes 304160 | tf_op jit(solution)/shard_map/ecr,rd->ecd/dot_general | solution.py:34
  2.9 0.2 copy.20
  3.1 17.2 %all_to_all.29 = bf16[16,4,2048]{2,1,0:T(4,128)(2,1)S(1)} all-to-all(bf16[16,4,2048]{2,1,0:T(4,128)(2,1)S(1)} %copy.20), channel_id=1, replica_groups=mesh['grp'=2,'ep'=16] {'ep'}, dimensions={0} | all-to-all | bytes 524288 | tf_op jit(solution)/shard_map/all_to_all | solution.py:37
  20.4 0.1 reshape.32
  20.4 2.1 %fusion.3 = f32[64,512]{1,0:T(8,128)S(1)} fusion(bf16[64,2048]{1,0:T(8,128)(2,1)S(1)} %reshape.32, bf16[1,2048,512]{2,1,0:T(8,128)(2,1)} %param.13), kind=kOutput, calls=%fused_computation.6 | convolution fusion | flops 134217728 | bytes 2490368 | tf_op jit(solution)/shard_map/dot_general | solution.py:8
  22.5 0.0 copy-done
  22.5 0.0 copy-start.1
  22.5 2.5 %convolution_convert_fusion = bf16[64,2048]{1,0:T(8,128)(2,1)S(1)} fusion(bf16[1,512,2048]{2,1,0:T(8,128)(2,1)S(1)} %copy-done, bf16[64,2048]{1,0:T(8,128)(2,1)S(1)} %reshape.32, bf16[1,2048,512]{2,1,0:T(8,128)(2,1)} %param.14, f32[64,512]{1,0:T(8,128)S(1)} %fusion.3), kind=kOutput, calls=%fused_computation | convolution fusion | flops 268763136 | bytes 4849664 | tf_op jit(solution)/shard_map/dot_general | solution.py:11
  25.0 0.1 reshape.33
  25.1 12.7 %all_to_all.30 = bf16[16,4,2048]{2,1,0:T(4,128)(2,1)S(1)} all-to-all(bf16[16,4,2048]{2,1,0:T(4,128)(2,1)S(1)} %reshape.33), channel_id=1, replica_groups=mesh['grp'=2,'ep'=16] {'ep'}, dimensions={0} | all-to-all | bytes 524288 | tf_op jit(solution)/shard_map/all_to_all | solution.py:40
  37.8 0.6 %multiply_reduce_fusion = (f32[8]{0:T(128)S(1)}, f32[8,2048]{1,0:T(8,128)S(1)}) fusion(bf16[16,4,2048]{2,1,0:T(4,128)(2,1)S(1)} %all_to_all.30, f32[16,8]{0,1:T(8,128)S(1)} %bitcast.34, f32[16,8]{0,1:T(8,128)S(1)} %bitcast.33, s32[16,8]{0,1:T(8,128)S(1)} %add_bitcast_fusion), kind=kOutput, calls=%fused_computation.22 | convolution fusion | flops 12617208 | bytes 329248 | tf_op jit(solution)/shard_map/ecr,ecd->rd/dot_general | solution.py:44
  38.4 0.0 copy-done.1
  38.4 0.1 fusion.23
  38.5 9.3 %all_to_all.31 = bf16[8,16,128]{2,0,1:T(8,128)(2,1)S(1)} all-to-all(bf16[8,16,128]{2,0,1:T(8,128)(2,1)S(1)} %fusion.23), channel_id=1, replica_groups=mesh['grp'=2,'ep'=16] {'ep'}, dimensions={1} | all-to-all | bytes 65536 | tf_op jit(solution)/shard_map/all_to_all | solution.py:49
  47.8 0.6 %copy.27 = bf16[128,128]{1,0:T(8,128)(2,1)} copy(bf16[128,128]{1,0:T(8,128)(2,1)S(1)} %bitcast.31) | data formatting | bytes 65536
  (4 shorter events, 0.1 us)
Async XLA Ops:
  0.0 22.5 %copy-start = (bf16[1,512,2048]{2,1,0:T(8,128)(2,1)S(1)}, bf16[1,512,2048]{2,1,0:T(8,128)(2,1)}, u32[]{:S(2)}) copy-start(bf16[1,512,2048]{2,1,0:T(8,128)(2,1)} %param.15) | copy-start | bytes 6291460
  22.5 15.9 %copy-start.1 = (f32[2048]{0:T(1024)S(1)}, f32[2048]{0:T(1024)}, u32[]{:S(2)}) copy-start(f32[2048]{0:T(1024)} %param.12) | copy-start | bytes 24580
where the time goes:
time: 48.8 us; the launch traced here: 48.4 us
  blocking collectives  39.2 us (80%)
  matrix products  6.16 us (13%)
  other arithmetic  1.95 us (4%)
  local copies, waits for them, and re-layouts  1 us (2%)
    all_to_all x1, blocking collectives, shards(): lax.all_to_all(outgoing, 'ep', split_axis=0, concat_axis=0, tiled=True)  17.2 us
    all_to_all x1, blocking collectives, shards(): lax.all_to_all(result.reshape(group, count, width), 'ep', split_axis=0, c...  12.7 us
    all_to_all x1, blocking collectives, shards(): lax.all_to_all(finished, 'ep', split_axis=1, concat_axis=0, tiled=True)  9.31 us
    dot_general x1, matrix products, expert_rows(): jnp.dot(act, w_down[0], preferred_element_type=jnp.float32)  2.51 us
    dot_general x1, matrix products, expert_rows(): gate_val = jnp.dot(rows, w_gate[0], preferred_element_type=jnp.float32)  2.06 us
    reduce_sum x1, other arithmetic, shards(): jnp.mean(values * values, axis=1, keepdims=True) + epsilon  1.04 us
    dot_general x1, matrix products, shards(): jnp.einsum('ecr,rd->ecd', select.astype(jnp.bfloat16), normed, preferred_...  1.03 us

commit v1 on v0

v1 whole, which is shorter than its diff:
```python
import functools

import jax
import jax.numpy as jnp
from jax import lax
from jax.experimental import pallas as pl
from jax.experimental.pallas import tpu as pltpu
from jax.sharding import PartitionSpec as P

MESH = pl.DeviceIdType.MESH
BF16 = jnp.bfloat16
F32 = jnp.float32
NT = (((1,), (1,)), ((), ()))


def each(count, step):
    if count <= 16:
        for i in range(count):
            step(i)
    else:
        lax.fori_loop(0, count, lambda i, c: (step(i), c)[1], 0)


def far_first(i, n):
    half = (i + 1) // 2
    return n // 2 + half * (2 * (i % 2) - 1) * -1


def kernel(n, most, chunks, group, tokens, routes, gates, ngain, fgain, wg, wu, wd, out,
           wg_v, wu_v, wd_v, slots, recv, gate_own, gate_all, act_v, y_v, back, mix, sums_own, sums,
           w_sem, d_sem, s_send, s_recv, g_send, g_recv, y_send, y_recv, q_send, q_recv):
    me = lax.axis_index("ep")
    rows, width = tokens.shape
    topk = routes.shape[1]
    lanes = n * most
    part = width // chunks
    cols = width // n
    total = n * rows
    eps = 1e-06

    def peer(i):
        return lax.rem(me + far_first(i, n), n)

    def weight_copies(k):
        span = pl.ds(k * part, part)
        return (pltpu.make_async_copy(wg.at[0, span], wg_v.at[span], w_sem.at[k]),
                pltpu.make_async_copy(wu.at[0, span], wu_v.at[span], w_sem.at[chunks + k]))

    down_copy = pltpu.make_async_copy(wd.at[0], wd_v, d_sem)

    barrier = pltpu.get_barrier_semaphore()
    each(n - 1, lambda i: pl.semaphore_signal(barrier, inc=1, device_id={"ep": peer(i)}, device_id_type=MESH))
    for k in range(chunks):
        for c in weight_copies(k):
            c.start()
    down_copy.start()

    lane = lax.broadcasted_iota(jnp.int32, (rows, lanes), 1)
    lane_e, lane_c = lane // most, lane % most
    used = jnp.zeros((rows, lanes), F32)
    gate_of = jnp.zeros((rows, lanes), F32)
    for k in range(topk):
        hit = (routes[:, k:k + 1] == lane_e).astype(F32)
        used += hit
        gate_of += hit * gates[:, k:k + 1]
    row_a = lax.broadcasted_iota(jnp.int32, (rows, rows), 0)
    row_b = lax.broadcasted_iota(jnp.int32, (rows, rows), 1)
    before = jnp.dot((row_b < row_a).astype(F32), used, preferred_element_type=F32)
    select = jnp.where(before == lane_c.astype(F32), used, 0.0)
    weight = select * gate_of
    high = weight.astype(BF16)
    low = (weight - high.astype(F32)).astype(BF16)
    gate_own[...] = jnp.concatenate([high, low], axis=1)
    gate_all[me] = gate_own[...]

    values = tokens[...].astype(F32)
    normed = (values * lax.rsqrt(jnp.mean(values * values, axis=1, keepdims=True) + eps) * ngain[...]).astype(BF16)
    pick = jnp.transpose(select).astype(BF16)
    for k in range(chunks):
        sent = jnp.dot(pick, normed[:, k * part:(k + 1) * part], preferred_element_type=F32).astype(BF16)
        sent = sent.reshape(n, most, part)
        slots[k] = sent
        recv[k, me] = slots[k, me]

    pl.semaphore_wait(barrier, n - 1)
    for k in range(chunks):
        def dispatch(i, k=k):
            d = peer(i)
            pltpu.make_async_remote_copy(
                src_ref=slots.at[k, d], dst_ref=recv.at[k, me], send_sem=s_send.at[k], recv_sem=s_recv.at[k],
                device_id={"ep": d}, device_id_type=MESH).start()
        each(n - 1, dispatch)

    def share_gates(i):
        pltpu.make_async_remote_copy(
            src_ref=gate_own, dst_ref=gate_all.at[me], send_sem=g_send, recv_sem=g_recv,
            device_id={"ep": peer(i)}, device_id_type=MESH).start()
    each(n - 1, share_gates)

    def wait_bytes(ref, sem):
        pltpu.make_async_copy(ref, ref, sem).wait()

    gate_val = jnp.zeros((lanes, wg.shape[2]), F32)
    up_val = jnp.zeros((lanes, wg.shape[2]), F32)
    for k in range(chunks):
        for c in weight_copies(k):
            c.wait()
        wait_bytes(recv.at[k, pl.ds(0, n - 1)], s_recv.at[k])
        x = recv[k].reshape(lanes, part)
        gate_val += jnp.dot(x, wg_v[k * part:(k + 1) * part, :], preferred_element_type=F32)
        up_val += jnp.dot(x, wu_v[k * part:(k + 1) * part, :], preferred_element_type=F32)
    act_v[...] = (jax.nn.silu(gate_val) * up_val).astype(BF16)

    down_copy.wait()
    per = group // cols
    n_groups = width // group
    my_group = me // per

    def down(i):
        g = lax.rem(my_group + (far_first(i, n_groups) if n_groups > 1 else 0), n_groups)
        return g

    def project(g, own):
        y = jnp.dot(act_v[...], wd_v[:, pl.ds(pl.multiple_of(g * group, group), group)],
                    preferred_element_type=F32).astype(BF16)
        for j in range(per):
            d = g * per + j
            y_v[d] = y[:, j * cols:(j + 1) * cols]

            def send(d=d):
                pltpu.make_async_remote_copy(
                    src_ref=y_v.at[d], dst_ref=back.at[me], send_sem=y_send, recv_sem=y_recv,
                    device_id={"ep": d}, device_id_type=MESH).start()
            if own:
                pl.when(d != me)(send)
            else:
                send()
    each(n_groups - 1, lambda i: project(lax.rem(my_group + far_first(i, n_groups), n_groups), False))
    project(my_group, True)
    back[me] = y_v[me]

    wait_bytes(gate_all.at[pl.ds(0, n - 1)], g_recv)
    table = gate_all[...].reshape(total, 2 * lanes)
    tile = max(1, 256 // lanes) * lanes
    per_tile = tile // lanes

    def build(i):
        r = lax.broadcasted_iota(jnp.int32, (lanes, tile), 0)
        q = lax.broadcasted_iota(jnp.int32, (lanes, tile), 1)
        spread = (r == (i * per_tile + q // lanes) * most + q % most).astype(BF16)
        t = lax.broadcasted_iota(jnp.int32, (total, tile), 0)
        q2 = lax.broadcasted_iota(jnp.int32, (total, tile), 1)
        mine = (q2 % lanes) // most == t // rows
        for h in range(2):
            w = jnp.dot(table[:, h * lanes:(h + 1) * lanes], spread, preferred_element_type=F32)
            mix[i, h * total:(h + 1) * total] = jnp.where(mine, w, 0.0).astype(BF16)
    each(n // per_tile, build)

    wait_bytes(back.at[pl.ds(0, n - 1)], y_recv)
    both = jnp.zeros((2 * total, cols), F32)

    def gather(i, both):
        r = back[pl.ds(i * per_tile, per_tile)].reshape(tile, cols)
        return both + jnp.dot(mix[i], r, preferred_element_type=F32)
    if n <= 16:
        for i in range(n // per_tile):
            both = gather(i, both)
    else:
        both = lax.fori_loop(0, n // per_tile, gather, both)
    combined = both[:total] + both[total:]

    square = combined * combined
    ones = jnp.ones((8, cols), BF16)
    row = jnp.zeros((8, total), F32)
    for _ in range(3):
        piece = square.astype(BF16)
        row += lax.dot_general(ones, piece, NT, preferred_element_type=F32)
        square = square - piece.astype(F32)
    sums_own[...] = row[:1]
    sums[me] = sums_own[...]

    def share_sums(i):
        pltpu.make_async_remote_copy(
            src_ref=sums_own, dst_ref=sums.at[me], send_sem=q_send, recv_sem=q_recv,
            device_id={"ep": peer(i)}, device_id_type=MESH).start()
    each(n - 1, share_sums)

    per_lane = 128 // cols if cols < 128 else 1
    wide = cols * per_lane
    gain = fgain[:, pl.ds(pl.multiple_of((me // per_lane) * wide, wide), wide)]
    if per_lane > 1:
        gain = functools.reduce(jnp.add, [
            jnp.where(lax.rem(me, per_lane) == j, gain[:, j * cols:(j + 1) * cols], 0.0) for j in range(per_lane)])

    wait_bytes(sums.at[pl.ds(0, n - 1)], q_recv)
    mean = jnp.sum(sums[...], axis=0) * (1.0 / width)
    scale = jnp.transpose(jnp.broadcast_to(lax.rsqrt(mean + eps), (128, total)))
    out[...] = (combined * scale[:, :1] * gain).astype(BF16)

    for k in range(chunks):
        wait_bytes(slots.at[k, pl.ds(0, n - 1)], s_send.at[k])
    wait_bytes(gate_all.at[pl.ds(0, n - 1)], g_send)
    wait_bytes(y_v.at[pl.ds(0, n - 1)], y_send)
    wait_bytes(sums.at[pl.ds(0, n - 1)], q_send)


def shards(tokens, routes, gate_weights, norm_gain, final_gain, w_gate, w_up, w_down):
    n = lax.axis_size("ep")
    rows, width = tokens.shape
    topk = routes.shape[1]
    ff = w_gate.shape[2]
    most = max(2, (2 * rows * topk + n - 1) // n)
    lanes = n * most
    chunks = 4
    cols = width // n
    group = max(256, cols)
    total = n * rows
    tile = max(1, 256 // lanes) * lanes
    vmem = pl.BlockSpec(memory_space=pltpu.VMEM)
    hbm = pl.BlockSpec(memory_space=pl.ANY)
    dma = pltpu.SemaphoreType.DMA
    return pl.pallas_call(
        functools.partial(kernel, n, most, chunks, group),
        out_shape=jax.ShapeDtypeStruct((total, cols), BF16),
        in_specs=[vmem] * 5 + [hbm] * 3,
        out_specs=vmem,
        scratch_shapes=[
            pltpu.VMEM((width, ff), BF16),
            pltpu.VMEM((width, ff), BF16),
            pltpu.VMEM((ff, width), BF16),
            pltpu.VMEM((chunks, n, most, width // chunks), BF16),
            pltpu.VMEM((chunks, n, most, width // chunks), BF16),
            pltpu.VMEM((rows, 2 * lanes), BF16),
            pltpu.VMEM((n, rows, 2 * lanes), BF16),
            pltpu.VMEM((lanes, ff), BF16),
            pltpu.VMEM((n, lanes, cols), BF16),
            pltpu.VMEM((n, lanes, cols), BF16),
            pltpu.VMEM((n * lanes // tile, 2 * total, tile), BF16),
            pltpu.VMEM((1, total), F32),
            pltpu.VMEM((n, 1, total), F32),
            dma((2 * chunks,)), dma, dma((chunks,)), dma((chunks,)),
            dma, dma, dma, dma, dma, dma,
        ],
        compiler_params=pltpu.CompilerParams(collective_id=0, has_side_effects=True, vmem_limit_bytes=56 * 2**20),
    )(tokens, routes, gate_weights, norm_gain.reshape(1, width), final_gain.reshape(1, width), w_gate, w_up, w_down)


def solution(mesh):
    in_specs = (
        P(("grp", "ep"), None),
        P(("grp", "ep"), None),
        P(("grp", "ep"), None),
        P(),
        P(),
        P("ep", None, None),
        P("ep", None, None),
        P("ep", None, None),
    )
    out_specs = P("grp", "ep")
    return jax.shard_map(shards, mesh=mesh, in_specs=in_specs, out_specs=out_specs, check_vma=False)
```

time: 48.8 us -> 32.1 us (0.66)
  blocking collectives: 39.2 us -> 0 us
  Pallas kernels: 0 us -> 27.8 us
  matrix products: 6.16 us -> 0 us
  local copies, waits for them, and re-layouts: 1 us -> 4.06 us
  other arithmetic: 1.95 us -> 0 us
    all_to_all x3 -> x0, blocking collectives: 39.2 us -> none  [the longest x1 17.2 us: shards(): lax.all_to_all(outgoing, 'ep', split_axis=0, concat_axis=0, tiled=True)]
    pallas_call x0 -> x1, Pallas kernels: none -> 27.8 us  [shards(): pl.pallas_call(functools.partial(kernel, n, most, chunks, group), out_sha...]
    dot_general x4 -> x0, matrix products: 6.16 us -> none  [the longest x1 2.51 us: expert_rows(): jnp.dot(act, w_down[0], preferred_element_type=jnp.float32)]
    unnamed x5 -> x3, local copies, waits for them, and re-layouts: 0.63 us -> 4.06 us
    reduce_sum x2 -> x0, other arithmetic: 1.82 us -> none  [the longest x1 1.04 us: shards(): jnp.mean(values * values, axis=1, keepdims=True) + epsilon]
where the time goes in v1:
time: 32.1 us; the launch traced here: 31.8 us
  Pallas kernels  27.8 us (87%)
  local copies, waits for them, and re-layouts  4.06 us (13%)
    pallas_call x1, Pallas kernels, shards(): pl.pallas_call(functools.partial(kernel, n, most, chunks, group), out_sha...  27.8 us
    unnamed x3, local copies, waits for them, and re-layouts  4.06 us

profile of v1, /device:TPU:0, one launch (start us, length us, event | category | flops | bytes accessed | tf_op | source)
XLA Modules:
  0.0 31.8 jit_solution(2662021959541216064)
XLA Ops:
  0.0 1.3 %copy.9.routes = s32[8,4]{1,0:T(8,128)} copy(s32[8,4]{0,1:T(4,128)} %param.9) | data formatting | bytes 256 | tf_op args[1]
  1.3 1.3 %copy.10.gates = f32[8,4]{1,0:T(8,128)} copy(f32[8,4]{0,1:T(4,128)} %param.10) | data formatting | bytes 256 | tf_op args[2]
  2.7 27.8 %shard_map.82 = bf16[128,128]{1,0:T(8,128)(2,1)} custom-call(bf16[8,2048]{1,0:T(8,128)(2,1)} %tokens.1, s32[8,4]{1,0:T(8,128)} %copy.9.routes, f32[8,4]{1,0:T(8,128)} %copy.10.gates, f32[1,2048]{1,0:T(1,128)} %bitcast.2, f32[1,2048]{1,0:T(1,128)} %bitcast.3, bf16[1,2048,512]{2,1,0:T(8,128)(2,1)} %wg.1, bf16[1,2048,512]{2,1,0:T(8,128)(2,1)} %wu.1, ...), custom_call_target="tpu_custom_call" | custom-call | tf_op jit(solution)/shard_map/pallas_call | solution.py:222
  30.5 1.4 %copy.12 = bf16[128,128]{1,0:T(8,128)(2,1)} copy(bf16[128,128]{1,0:T(8,128)(2,1)} %shard_map.82) | data formatting | bytes 65536

commit v2 on v1

--- a/solution.py
+++ b/solution.py
@@ -31,7 +31,7 @@
            w_sem, d_sem, s_send, s_recv, g_send, g_recv, y_send, y_recv, q_send, q_recv):
     me = lax.axis_index("ep")
     rows, width = tokens.shape
-    topk = routes.shape[1]
+    topk = routes.shape[0]
     lanes = n * most
     part = width // chunks
     cols = width // n
@@ -55,32 +55,32 @@
             c.start()
     down_copy.start()
 
-    lane = lax.broadcasted_iota(jnp.int32, (rows, lanes), 1)
-    lane_e, lane_c = lane // most, lane % most
-    used = jnp.zeros((rows, lanes), F32)
-    gate_of = jnp.zeros((rows, lanes), F32)
+    slot = lax.broadcasted_iota(jnp.int32, (lanes, rows), 0)
+    slot_e, slot_c = slot // most, slot % most
+    used = jnp.zeros((lanes, rows), F32)
+    gate_of = jnp.zeros((lanes, rows), F32)
     for k in range(topk):
-        hit = (routes[:, k:k + 1] == lane_e).astype(F32)
+        hit = (routes[k:k + 1, :] == slot_e).astype(F32)
         used += hit
-        gate_of += hit * gates[:, k:k + 1]
+        gate_of += hit * gates[k:k + 1, :]
     row_a = lax.broadcasted_iota(jnp.int32, (rows, rows), 0)
     row_b = lax.broadcasted_iota(jnp.int32, (rows, rows), 1)
-    before = jnp.dot((row_b < row_a).astype(F32), used, preferred_element_type=F32)
-    select = jnp.where(before == lane_c.astype(F32), used, 0.0)
-    weight = select * gate_of
+    before = jnp.dot(used, (row_a < row_b).astype(F32), preferred_element_type=F32)
+    select = jnp.where(before == slot_c.astype(F32), used, 0.0)
+    pick = select.astype(BF16)
+
+    values = tokens[...].astype(F32)
+    normed = (values * lax.rsqrt(jnp.mean(values * values, axis=1, keepdims=True) + eps) * ngain[...]).astype(BF16)
+    for k in range(chunks):
+        sent = jnp.dot(pick, normed[:, k * part:(k + 1) * part], preferred_element_type=F32).astype(BF16)
+        sent = sent.reshape(n, most, part)
+        slots[k] = sent
+        recv[k, me] = slots[k, me]
+    weight = jnp.transpose(select * gate_of)
     high = weight.astype(BF16)
     low = (weight - high.astype(F32)).astype(BF16)
     gate_own[...] = jnp.concatenate([high, low], axis=1)
     gate_all[me] = gate_own[...]
-
-    values = tokens[...].astype(F32)
-    normed = (values * lax.rsqrt(jnp.mean(values * values, axis=1, keepdims=True) + eps) * ngain[...]).astype(BF16)
-    pick = jnp.transpose(select).astype(BF16)
-    for k in range(chunks):
-        sent = jnp.dot(pick, normed[:, k * part:(k + 1) * part], preferred_element_type=F32).astype(BF16)
-        sent = sent.reshape(n, most, part)
-        slots[k] = sent
-        recv[k, me] = slots[k, me]
 
     pl.semaphore_wait(barrier, n - 1)
     for k in range(chunks):
@@ -242,7 +242,7 @@
             dma, dma, dma, dma, dma, dma,
         ],
         compiler_params=pltpu.CompilerParams(collective_id=0, has_side_effects=True, vmem_limit_bytes=56 * 2**20),
-    )(tokens, routes, gate_weights, norm_gain.reshape(1, width), final_gain.reshape(1, width), w_gate, w_up, w_down)
+    )(tokens, routes.T, gate_weights.T, norm_gain.reshape(1, width), final_gain.reshape(1, width), w_gate, w_up, w_down)
 
 
 def solution(mesh):

time: 32.1 us -> 29.4 us (0.916)
  local copies, waits for them, and re-layouts: 4.06 us -> 1.38 us
    unnamed x3 -> x1, local copies, waits for them, and re-layouts: 4.06 us -> 1.38 us
where the time goes in v2:
time: 29.4 us; the launch traced here: 29.1 us
  Pallas kernels  27.7 us (94%)
  local copies, waits for them, and re-layouts  1.38 us (5%)
    pallas_call x1, Pallas kernels, shards(): pl.pallas_call(functools.partial(kernel, n, most, chunks, group), out_sha...  27.7 us
    unnamed x1, local copies, waits for them, and re-layouts  1.38 us

profile of v2, /device:TPU:0, one launch (start us, length us, event | category | flops | bytes accessed | tf_op | source)
XLA Modules:
  0.0 29.1 jit_solution(6511355729516405843)
XLA Ops:
  0.0 27.7 %shard_map.82 = bf16[128,128]{1,0:T(8,128)(2,1)} custom-call(bf16[8,2048]{1,0:T(8,128)(2,1)} %tokens.1, s32[4,8]{1,0:T(4,128)} %bitcast.6, f32[4,8]{1,0:T(4,128)} %bitcast.7, f32[1,2048]{1,0:T(1,128)} %bitcast.4, f32[1,2048]{1,0:T(1,128)} %bitcast.5, bf16[1,2048,512]{2,1,0:T(8,128)(2,1)} %wg.1, bf16[1,2048,512]{2,1,0:T(8,128)(2,1)} %wu.1, ...), custom_call_target="tpu_custom_call" | custom-call | tf_op jit(solution)/shard_map/pallas_call | solution.py:222
  27.7 1.4 %copy.10 = bf16[128,128]{1,0:T(8,128)(2,1)} copy(bf16[128,128]{1,0:T(8,128)(2,1)} %shard_map.82) | data formatting | bytes 65536

commit v3 on v2

--- a/solution.py
+++ b/solution.py
@@ -26,7 +26,8 @@
     return n // 2 + half * (2 * (i % 2) - 1) * -1
 
 
-def kernel(n, most, chunks, group, tokens, routes, gates, ngain, fgain, wg, wu, wd, out,
+def kernel(n, most, chunks, group, tokens_in, routes_in, gates_in, ngain_in, fgain_in, wg, wu, wd, out,
+           tokens, routes, gates, ngain, fgain, in_sem,
            wg_v, wu_v, wd_v, slots, recv, gate_own, gate_all, act_v, y_v, back, mix, sums_own, sums,
            w_sem, d_sem, s_send, s_recv, g_send, g_recv, y_send, y_recv, q_send, q_recv):
     me = lax.axis_index("ep")
@@ -50,10 +51,16 @@
 
     barrier = pltpu.get_barrier_semaphore()
     each(n - 1, lambda i: pl.semaphore_signal(barrier, inc=1, device_id={"ep": peer(i)}, device_id_type=MESH))
+    small = [pltpu.make_async_copy(a, b, in_sem.at[i]) for i, (a, b) in enumerate((
+        (tokens_in, tokens), (routes_in, routes), (gates_in, gates), (ngain_in, ngain), (fgain_in, fgain)))]
+    for c in small:
+        c.start()
     for k in range(chunks):
         for c in weight_copies(k):
             c.start()
     down_copy.start()
+    for c in small:
+        c.wait()
 
     slot = lax.broadcasted_iota(jnp.int32, (lanes, rows), 0)
     slot_e, slot_c = slot // most, slot % most
@@ -222,9 +229,15 @@
     return pl.pallas_call(
         functools.partial(kernel, n, most, chunks, group),
         out_shape=jax.ShapeDtypeStruct((total, cols), BF16),
-        in_specs=[vmem] * 5 + [hbm] * 3,
+        in_specs=[hbm] * 8,
         out_specs=vmem,
         scratch_shapes=[
+            pltpu.VMEM((rows, width), BF16),
+            pltpu.VMEM((topk, rows), jnp.int32),
+            pltpu.VMEM((topk, rows), F32),
+            pltpu.VMEM((1, width), F32),
+            pltpu.VMEM((1, width), F32),
+            dma((5,)),
             pltpu.VMEM((width, ff), BF16),
             pltpu.VMEM((width, ff), BF16),
             pltpu.VMEM((ff, width), BF16),

time: 29.4 us -> 29 us (0.986)
  no operation moved by 1% of the time
where the time goes in v3:
time: 29 us; the launch traced here: 28.8 us
  Pallas kernels  27.5 us (95%)
  local copies, waits for them, and re-layouts  1.38 us (5%)
    pallas_call x1, Pallas kernels, shards(): pl.pallas_call(functools.partial(kernel, n, most, chunks, group), out_sha...  27.5 us
    unnamed x1, local copies, waits for them, and re-layouts  1.38 us

profile of v3, /device:TPU:0, one launch (start us, length us, event | category | flops | bytes accessed | tf_op | source)
XLA Modules:
  0.0 28.8 jit_solution(5858002632653828615)
XLA Ops:
  0.0 27.5 %shard_map.82 = bf16[128,128]{1,0:T(8,128)(2,1)} custom-call(bf16[8,2048]{1,0:T(8,128)(2,1)} %tokens_in.1, s32[4,8]{1,0:T(4,128)} %bitcast.6, f32[4,8]{1,0:T(4,128)} %bitcast.7, f32[1,2048]{1,0:T(1,128)} %bitcast.4, f32[1,2048]{1,0:T(1,128)} %bitcast.5, bf16[1,2048,512]{2,1,0:T(8,128)(2,1)} %wg.1, bf16[1,2048,512]{2,1,0:T(8,128)(2,1)} %wu.1, ...), custom_call_target="tpu_custom_call" | custom-call | tf_op jit(solution)/shard_map/pallas_call | solution.py:229
  27.5 1.4 %copy.10 = bf16[128,128]{1,0:T(8,128)(2,1)} copy(bf16[128,128]{1,0:T(8,128)(2,1)} %shard_map.82) | data formatting | bytes 65536
